TPU v7x, 32 devices: a whole 2x2x4 slice. The times are simulated.
32 devices in a mesh: fs: 16 (over z, y, x), tp: 2 (over core).
Axes of the slice: x: 2, y: 2, z: 4, core: 2. Of those that a mesh axis runs over, the one named last changes fastest.
Arguments:
- tokens: bfloat16 [12288, 2048], P('fs'), may hold values from -6 to 6
- norm_gain: float32 [2048], replicated, may hold values from 0.1 to 1.9
- gate_weight: bfloat16 [2048, 5120], P('fs', 'tp'), may hold values from -0.125 to 0.125
- up_weight: bfloat16 [2048, 5120], P('fs', 'tp'), may hold values from -0.125 to 0.125
- down_weight: bfloat16 [5120, 2048], P('tp', 'fs'), may hold values from -0.078125 to 0.078125
Outputs:
- mixed: bfloat16 [12288, 2048], P(('fs', 'tp'))
All inputs are finite; a program needn't handle non-finite values.
Results may differ from a plain program's by a relative error of at most 0.014.
Values may be sent and summed in bfloat16 or wider, within the bound.
A program may use at most 128 MiB of HBM per device.

v0:
```python
import jax
import jax.numpy as jnp
from jax import lax
from jax.sharding import PartitionSpec as P


def add_rows(normed, piece):
    return jnp.dot(normed, piece, preferred_element_type=jnp.float32)


def per_device(tokens, norm_gain, gate_weight, up_weight, down_weight):
    values = tokens.astype(jnp.float32)
    scale = lax.rsqrt(jnp.mean(values * values, axis=-1, keepdims=True) + 1e-06)
    normed = (values * scale * norm_gain).astype(jnp.bfloat16)

    def add_single(piece):
        return add_rows(normed, piece)

    gate_proj = add_single(lax.all_gather(gate_weight, "fs", axis=0, tiled=True))
    up_proj = add_single(lax.all_gather(up_weight, "fs", axis=0, tiled=True))
    hidden = (jax.nn.silu(gate_proj) * up_proj).astype(jnp.bfloat16)
    down_whole = lax.all_gather(down_weight, "fs", axis=1, tiled=True)
    return lax.psum_scatter(
        jnp.dot(hidden, down_whole, preferred_element_type=jnp.float32).astype(jnp.bfloat16),
        "tp",
        scatter_dimension=0,
        tiled=True,
    )


def solution(mesh):
    in_specs = (P("fs", None), P(), P("fs", "tp"), P("fs", "tp"), P("tp", "fs"))
    out_specs = P(("fs", "tp"), None)
    return jax.shard_map(
        per_device, mesh=mesh, in_specs=in_specs, out_specs=out_specs, check_vma=False
    )
```

profile of v0, /device:TPU:0, one launch (start us, length us, event | category | flops | bytes accessed | tf_op | source)
XLA Modules:
  0.0 489.8 jit_solution(3628427633222220995)
XLA Ops:
  6.5 0.0 all-gather.4.cloned.1.call-start
  6.5 0.7 all-gather.4.cloned.1.call-update
  7.3 0.0 all-gather.6.cloned.1.call-start
  7.3 0.7 all-gather.6.cloned.1.call-update
  8.0 0.0 all-gather.8.cloned.1.call-start
  8.1 0.7 all-gather.8.cloned.1.call-update
  8.7 0.0 reduce-scatter.2.cloned.1.call-start
  8.8 2.6 fusion
  11.4 0.0 copy-start
  11.4 0.0 copy-start.1
  11.4 132.8 %all-gather.4.cloned.1.call-done = bf16[2048,2560]{1,0:T(8,128)(2,1)} async-done(((bf16[128,2560]{1,0:T(8,128)(2,1)}), bf16[2048,2560]{1,0:T(8,128)(2,1)}) %all-gather.4.cloned.1.call-update) | async-done | bytes 10485776 | tf_op jit(solution)/shard_map/all_gather | solution.py:19
  144.2 13.9 %fusion.5 = f32[768,2560]{1,0:T(8,128)} fusion(bf16[2048,2560]{1,0:T(8,128)(2,1)} %all-gather.4.cloned.1.call-done, bf16[768,2048]{1,0:T(8,128)(2,1)} %param.5, f32[2048]{0:T(1024)} %param.6, f32[768]{0:T(1024)S(1)} %add_rsqrt_fusion), kind=kOutput, calls=%fused_computation.7 | convolution fusion | flops 8059355136 | bytes 21507072 | tf_op jit(solution)/shard_map/dot_general | solution.py:8
  158.2 118.4 %all-gather.6.cloned.1.call-done = bf16[2048,2560]{1,0:T(8,128)(2,1)} async-done(((bf16[128,2560]{1,0:T(8,128)(2,1)}), bf16[2048,2560]{1,0:T(8,128)(2,1)}) %all-gather.6.cloned.1.call-update) | async-done | bytes 10485776 | tf_op jit(solution)/shard_map/all_gather | solution.py:20
  276.6 169.6 %all-gather.8.cloned.1.call-done = bf16[2560,2048]{1,0:T(8,128)(2,1)} async-done(((bf16[2560,128]{1,0:T(8,128)(2,1)}), bf16[2560,2048]{1,0:T(8,128)(2,1)}) %all-gather.8.cloned.1.call-update) | async-done | bytes 10485776 | tf_op jit(solution)/shard_map/all_gather | solution.py:22
  446.2 0.0 copy-done
  446.2 0.0 copy-done.1
  446.2 27.6 %convolution_convert_fusion = bf16[768,2048]{1,0:T(8,128)(2,1)} fusion(bf16[2560,2048]{1,0:T(8,128)(2,1)} %all-gather.8.cloned.1.call-done, f32[768,2560]{1,0:T(8,128)} %fusion.5, bf16[2048,2560]{1,0:T(8,128)(2,1)} %all-gather.6.cloned.1.call-done, bf16[768,2048]{1,0:T(8,128)(2,1)S(1)} %copy-done, f32[2048]{0:T(1024)S(1)} %copy-done.1, ...), kind=kOutput, calls=%fused_computation.6 | convolution fusion | flops 16125788160 | bytes 35138560 | tf_op jit(solution)/shard_map/dot_general | solution.py:24
  473.8 0.0 reduce-scatter.2.cloned.1.call-update
  473.8 9.5 %reduce-scatter.2.cloned.1.call-done = bf16[384,2048]{1,0:T(8,128)(2,1)} async-done(((bf16[768,2048]{1,0:T(8,128)(2,1)}), bf16[384,2048]{1,0:T(8,128)(2,1)}) %reduce-scatter.2.cloned.1.call-update) | async-done | bytes 1572880 | tf_op jit(solution)/shard_map/reduce_scatter | solution.py:23
  (1 shorter events, 0.0 us)
Async XLA Ops:
  6.5 137.7 %all-gather.4.cloned.1.call-start = ((), (), s32[]{:S(2)}) async-start(), calls=%async_computation.1 | async-start | bytes 11141120 | tf_op jit(solution)/shard_map/all_gather | solution.py:19
  7.3 269.4 %all-gather.6.cloned.1.call-start = ((), (), s32[]{:S(2)}) async-start(), calls=%async_computation.2 | async-start | bytes 11141120 | tf_op jit(solution)/shard_map/all_gather | solution.py:20
  8.0 438.2 %all-gather.8.cloned.1.call-start = ((), (), s32[]{:S(2)}) async-start(), calls=%async_computation.3 | async-start | bytes 11141120 | tf_op jit(solution)/shard_map/all_gather | solution.py:22
  8.7 474.6 %reduce-scatter.2.cloned.1.call-start = ((), (), s32[]{:S(2)}) async-start(), calls=%async_computation.4 | async-start | bytes 4718592 | tf_op jit(solution)/shard_map/reduce_scatter | solution.py:23
  11.4 434.8 %copy-start = (bf16[768,2048]{1,0:T(8,128)(2,1)S(1)}, bf16[768,2048]{1,0:T(8,128)(2,1)}, u32[]{:S(2)}) copy-start(bf16[768,2048]{1,0:T(8,128)(2,1)} %param.5) | copy-start | bytes 9437188
  11.4 434.8 %copy-start.1 = (f32[2048]{0:T(1024)S(1)}, f32[2048]{0:T(1024)}, u32[]{:S(2)}) copy-start(f32[2048]{0:T(1024)} %param.6) | copy-start | bytes 24580
Sparse Core Ops, SparseCore 0:
  10.0 134.1 all-gather.3
  146.9 129.6 all-gather.5
  279.3 166.8 all-gather.7
  473.9 9.3 reduce-scatter.1
where the time goes:
time: 490 us
  waiting for transfers between devices  432 us (88%)
  matrix products  41.5 us (8%)
  between operations  13.1 us (3%)
    all_gather x1, waiting for transfers between devices, per_device(): down_whole = lax.all_gather(down_weight, 'fs', axis=1, tiled=True)  170 us
    all_gather x1, waiting for transfers between devices, per_device(): lax.all_gather(gate_weight, 'fs', axis=0, tiled=True)  133 us
    all_gather x1, waiting for transfers between devices, per_device(): up_proj = add_single(lax.all_gather(up_weight, 'fs', axis=0, tiled=True))  118 us
    dot_general x1, matrix products, per_device(): jnp.dot(hidden, down_whole, preferred_element_type=jnp.float32)  27.6 us
    dot_general x1, matrix products, add_rows(): return jnp.dot(normed, piece, preferred_element_type=jnp.float32)  13.9 us
  transfers between devices with their start and end apart: 4, of which 4 were waited for; matrix products, arithmetic and copies ran while one was open for 3% of the time, Pallas kernels for 0%

commit v1 on v0

--- a/solution.py
+++ b/solution.py
@@ -19,7 +19,8 @@
     gate_proj = add_single(lax.all_gather(gate_weight, "fs", axis=0, tiled=True))
     up_proj = add_single(lax.all_gather(up_weight, "fs", axis=0, tiled=True))
     hidden = (jax.nn.silu(gate_proj) * up_proj).astype(jnp.bfloat16)
-    down_whole = lax.all_gather(down_weight, "fs", axis=1, tiled=True)
+    shards = lax.all_gather(down_weight, "fs", axis=0, tiled=False)
+    down_whole = jnp.concatenate(shards, axis=1)
     return lax.psum_scatter(
         jnp.dot(hidden, down_whole, preferred_element_type=jnp.float32).astype(jnp.bfloat16),
         "tp",

time: 490 us -> 451 us (0.920)
  waiting for transfers between devices: 432 us -> 382 us
  local copies, waits for them, and re-layouts: 0.01 us -> 14.2 us
    all_gather x1, waiting for transfers between devices: 170 us -> 133 us  [per_device(): shards = lax.all_gather(down_weight, 'fs', axis=0, tiled=False)]
    all_gather x1, waiting for transfers between devices: 133 us -> 118 us  [per_device(): lax.all_gather(gate_weight, 'fs', axis=0, tiled=True)]
    reshape x0 -> x1, local copies, waits for them, and re-layouts: none -> 14.2 us  [per_device(): down_whole = jnp.concatenate(shards, axis=1)]
  transfers between devices with their start and end apart: 4 -> 4, of which waited for: 4 -> 4; matrix products, arithmetic and copies ran while one was open for 3% -> 7% of each run, Pallas kernels for 0% -> 0%
where the time goes in v1:
time: 451 us
  waiting for transfers between devices  382 us (85%)
  matrix products  38.9 us (9%)
  local copies, waits for them, and re-layouts  14.2 us (3%)
  between operations  13.1 us (3%)
    all_gather x1, waiting for transfers between devices, per_device(): shards = lax.all_gather(down_weight, 'fs', axis=0, tiled=False)  133 us
    all_gather x1, waiting for transfers between devices, per_device(): up_proj = add_single(lax.all_gather(up_weight, 'fs', axis=0, tiled=True))  119 us
    all_gather x1, waiting for transfers between devices, per_device(): lax.all_gather(gate_weight, 'fs', axis=0, tiled=True)  118 us
    dot_general x1, matrix products, per_device(): jnp.dot(hidden, down_whole, preferred_element_type=jnp.float32)  25.9 us
    reshape x1, local copies, waits for them, and re-layouts, per_device(): down_whole = jnp.concatenate(shards, axis=1)  14.2 us
    dot_general x1, matrix products, add_rows(): return jnp.dot(normed, piece, preferred_element_type=jnp.float32)  13 us
    reduce_scatter x1, waiting for transfers between devices, per_device(): lax.psum_scatter(jnp.dot(hidden, down_whole, preferred_element_type=jnp.f...  9.51 us
  transfers between devices with their start and end apart: 4, of which 4 were waited for; matrix products, arithmetic and copies ran while one was open for 7% of the time, Pallas kernels for 0%

profile of v1, /device:TPU:0, one launch (start us, length us, event | category | flops | bytes accessed | tf_op | source)
XLA Modules:
  0.0 451.0 jit_solution(9232343906918827705)
XLA Ops:
  6.5 0.0 all-gather.9.cloned.1.call-start
  6.5 0.7 all-gather.9.cloned.1.call-update
  7.3 0.0 all-gather.5.cloned.1.call-start
  7.3 0.7 all-gather.5.cloned.1.call-update
  8.0 0.0 all-gather.7.cloned.1.call-start
  8.1 0.7 all-gather.7.cloned.1.call-update
  8.7 0.0 reduce-scatter.2.cloned.1.call-start
  8.8 2.6 fusion
  11.4 132.9 %all-gather.9.cloned.1.call-done = bf16[40960,128]{1,0:T(8,128)(2,1)} async-done(((bf16[2560,128]{1,0:T(8,128)(2,1)}), bf16[40960,128]{1,0:T(8,128)(2,1)}) %all-gather.9.cloned.1.call-update) | async-done | bytes 10485776 | tf_op jit(solution)/shard_map/all_gather | solution.py:22
  144.2 0.0 copy-start
  144.2 0.0 copy-start.1
  144.2 14.2 %copy.6 = bf16[2560,16,128]{0,2,1:T(8,128)(2,1)} copy(bf16[2560,16,128]{2,0,1:T(8,128)(2,1)} %bitcast.7) | data formatting | bytes 20971520 | tf_op jit(solution)/shard_map/reshape | solution.py:23
  158.4 118.2 %all-gather.5.cloned.1.call-done = bf16[2048,2560]{1,0:T(8,128)(2,1)} async-done(((bf16[128,2560]{1,0:T(8,128)(2,1)}), bf16[2048,2560]{1,0:T(8,128)(2,1)}) %all-gather.5.cloned.1.call-update) | async-done | bytes 10485776 | tf_op jit(solution)/shard_map/all_gather | solution.py:19
  276.6 0.0 copy-done
  276.6 0.0 copy-done.1
  276.6 13.0 %fusion.5 = f32[768,2560]{1,0:T(8,128)} fusion(bf16[2048,2560]{1,0:T(8,128)(2,1)} %all-gather.5.cloned.1.call-done, bf16[768,2048]{1,0:T(8,128)(2,1)S(1)} %copy-done, f32[2048]{0:T(1024)S(1)} %copy-done.1, f32[768]{0:T(1024)S(1)} %add_rsqrt_fusion), kind=kOutput, calls=%fused_computation.7 | convolution fusion | flops 8059355136 | bytes 21507072 | tf_op jit(solution)/shard_map/dot_general | solution.py:8
  289.6 119.4 %all-gather.7.cloned.1.call-done = bf16[2048,2560]{1,0:T(8,128)(2,1)} async-done(((bf16[128,2560]{1,0:T(8,128)(2,1)}), bf16[2048,2560]{1,0:T(8,128)(2,1)}) %all-gather.7.cloned.1.call-update) | async-done | bytes 10485776 | tf_op jit(solution)/shard_map/all_gather | solution.py:20
  409.0 25.9 %convolution_convert_fusion = bf16[768,2048]{1,0:T(8,128)(2,1)} fusion(bf16[2560,2048]{0,1:T(8,128)(2,1)} %bitcast.8, f32[768,2560]{1,0:T(8,128)} %fusion.5, bf16[2048,2560]{1,0:T(8,128)(2,1)} %all-gather.7.cloned.1.call-done, bf16[768,2048]{1,0:T(8,128)(2,1)S(1)} %copy-done, f32[2048]{0:T(1024)S(1)} %copy-done.1, f32[768]{0:T(1024)S(1)} %add_rsqrt_fusion), kind=kOutput, calls=%fused_computation.6 | convolution fusion | flops 16125788160 | bytes 35138560 | tf_op jit(solution)/shard_map/dot_general | solution.py:25
  434.9 0.0 reduce-scatter.2.cloned.1.call-update
  434.9 9.5 %reduce-scatter.2.cloned.1.call-done = bf16[384,2048]{1,0:T(8,128)(2,1)} async-done(((bf16[768,2048]{1,0:T(8,128)(2,1)}), bf16[384,2048]{1,0:T(8,128)(2,1)}) %reduce-scatter.2.cloned.1.call-update) | async-done | bytes 1572880 | tf_op jit(solution)/shard_map/reduce_scatter | solution.py:24
  (1 shorter events, 0.0 us)
Async XLA Ops:
  6.5 137.7 %all-gather.9.cloned.1.call-start = ((), (), s32[]{:S(2)}) async-start(), calls=%async_computation.4 | async-start | bytes 11141120 | tf_op jit(solution)/shard_map/all_gather | solution.py:22
  7.3 269.4 %all-gather.5.cloned.1.call-start = ((), (), s32[]{:S(2)}) async-start(), calls=%async_computation.1 | async-start | bytes 11141120 | tf_op jit(solution)/shard_map/all_gather | solution.py:19
  8.0 401.0 %all-gather.7.cloned.1.call-start = ((), (), s32[]{:S(2)}) async-start(), calls=%async_computation.2 | async-start | bytes 11141120 | tf_op jit(solution)/shard_map/all_gather | solution.py:20
  8.7 435.7 %reduce-scatter.2.cloned.1.call-start = ((), (), s32[]{:S(2)}) async-start(), calls=%async_computation.3 | async-start | bytes 4718592 | tf_op jit(solution)/shard_map/reduce_scatter | solution.py:24
  144.2 132.4 %copy-start = (bf16[768,2048]{1,0:T(8,128)(2,1)S(1)}, bf16[768,2048]{1,0:T(8,128)(2,1)}, u32[]{:S(2)}) copy-start(bf16[768,2048]{1,0:T(8,128)(2,1)} %param.5) | copy-start | bytes 9437188
  144.2 132.4 %copy-start.1 = (f32[2048]{0:T(1024)S(1)}, f32[2048]{0:T(1024)}, u32[]{:S(2)}) copy-start(f32[2048]{0:T(1024)} %param.6) | copy-start | bytes 24580
Sparse Core Ops, SparseCore 0:
  10.0 134.1 all-gather.8
  146.9 129.6 all-gather.4
  279.3 129.6 all-gather.6
  435.0 9.3 reduce-scatter.1
